TPU v7x, 32 devices: a whole 2x2x4 slice. The times are simulated.
32 devices in a mesh: ep: 16 (over z, y, x), tp: 2 (over core).
Axes of the slice: x: 2, y: 2, z: 4, core: 2. Of those that a mesh axis runs over, the one named last changes fastest.
Arguments:
- tokens: bfloat16 [512, 2048], P('ep'), may hold values from -6 to 6
- mix_gain: float32 [2048], replicated, may hold values from 0.1 to 1.9
- w_query: bfloat16 [2048, 512], P('ep', 'tp'), may hold values from -0.125 to 0.125
- w_key: bfloat16 [2048, 512], P('ep', 'tp'), may hold values from -0.125 to 0.125
- w_value: bfloat16 [2048, 512], P('ep', 'tp'), may hold values from -0.125 to 0.125
- w_outgate: bfloat16 [2048, 512], P('ep', 'tp'), may hold values from -0.125 to 0.125
- w_igate: bfloat16 [2048, 8], P('ep', 'tp'), may hold values from -0.125 to 0.125
- w_fgate: bfloat16 [2048, 8], P('ep', 'tp'), may hold values from -0.125 to 0.125
- igate_bias: float32 [8], P('tp'), may hold values from -2 to 1
- fgate_bias: float32 [8], P('tp'), may hold values from 0 to 4
- head_gain: float32 [512], P('tp'), may hold values from 0.1 to 1.9
- w_out: bfloat16 [512, 2048], P('tp', 'ep'), may hold values from -0.25 to 0.25
- state_matrix: float32 [512, 8, 64, 64], P('ep', 'tp'), may hold values from -2.4 to 2.4
- state_norm: float32 [512, 8, 64], P('ep', 'tp'), may hold values from -2.4 to 2.4
- state_max: float32 [512, 8], P('ep', 'tp'), may hold values from -4 to 4
- ffn_gain: float32 [2048], replicated, may hold values from 0.1 to 1.9
- w_expert_gate: bfloat16 [16, 2048, 1408], P('ep', None, 'tp'), may hold values from -0.125 to 0.125
- w_expert_up: bfloat16 [16, 2048, 1408], P('ep', None, 'tp'), may hold values from -0.125 to 0.125
- w_expert_down: bfloat16 [16, 1408, 2048], P('ep', 'tp'), may hold values from -0.15625 to 0.15625
- routes: int32 [512, 3], P('ep'), may hold values from 0 to 15, all different within a row; in each aligned block of 32 rows (0 to 31, 32 to 63, ...) at most 12 rows name the same one
- route_weights: float32 [512, 3], P('ep'), may hold values from 0.2 to 1
Outputs:
- mixed: bfloat16 [512, 2048], P('ep')
- new_matrix: float32 [512, 8, 64, 64], P('ep', 'tp')
- new_norm: float32 [512, 8, 64], P('ep', 'tp')
- new_max: float32 [512, 8], P('ep', 'tp')
Inputs may be any that keep to these rules, and one draw needn't show every extreme that they name: `routes`: each row names 3 different experts. Among the rows of one device, no expert is named by more than 12 rows, a bound that some block reaches.
All inputs are finite; a program needn't handle non-finite values.
Results may differ from a plain program's by a relative error of at most 0.017.
Values may be sent and summed in bfloat16 or wider, within the bound.
No kernel may reach another device: no remote copies, remote signals or barrier semaphores. Data moves between devices by JAX's collectives and lax.ppermute only.
A program may use at most 128 MiB of HBM per device.

v0:
```python
import jax
import jax.numpy as jnp
from jax import lax
from jax.sharding import PartitionSpec as P


def rms_scale(values_in, gain_vec):
    widened = values_in.astype(jnp.float32)
    return (
        widened * lax.rsqrt(jnp.mean(widened * widened, axis=-1, keepdims=True) + 1e-06) * gain_vec
    )


def memory_cell(
    query,
    key_row,
    value_row,
    outgate,
    input_pre,
    forget_pre,
    head_gain,
    state_matrix,
    state_norm,
    state_max,
):
    seq_rows, head_count = input_pre.shape
    head_size = query.shape[1] // head_count
    query_heads = query.astype(jnp.float32).reshape(seq_rows, head_count, head_size)
    key_heads = key_row.astype(jnp.float32).reshape(
        seq_rows, head_count, head_size
    ) * head_size ** (-0.5)
    value_heads = value_row.astype(jnp.float32).reshape(seq_rows, head_count, head_size)
    log_forget = jax.nn.log_sigmoid(forget_pre)
    new_max = jnp.maximum(log_forget + state_max, input_pre)
    keep_old = jnp.exp(log_forget + state_max - new_max)
    keep_new = jnp.exp(input_pre - new_max)
    new_matrix = (
        keep_old[:, :, None, None] * state_matrix
        + keep_new[:, :, None, None] * value_heads[:, :, :, None] * key_heads[:, :, None, :]
    )
    new_norm = keep_old[:, :, None] * state_norm + keep_new[:, :, None] * key_heads
    numerator = jnp.sum(new_matrix * query_heads[:, :, None, :], axis=-1)
    denominator = jnp.sum(new_norm * query_heads, axis=-1)
    cell_read = numerator / jnp.maximum(jnp.abs(denominator), jnp.exp(-new_max))[:, :, None]
    centered = cell_read - jnp.mean(cell_read, axis=-1, keepdims=True)
    variance = jnp.mean(centered * centered, axis=-1, keepdims=True)
    scaled_cell = (centered * lax.rsqrt(variance + 1e-06)).reshape(seq_rows, head_count * head_size)
    cell_out = (scaled_cell * head_gain * jax.nn.sigmoid(outgate.astype(jnp.float32))).astype(
        jnp.bfloat16
    )
    return (cell_out, new_matrix, new_norm, new_max)


def torus_factors(count):
    side = 1
    while (2 * side) ** 3 <= count:
        side *= 2
    while count % (side * side):
        side -= 1
    return (count // (side * side), side, side)


def shift_pairs(factors, axis, step):
    pairs = []
    inner = 1
    for size in factors[axis + 1 :]:
        inner *= size
    total = factors[0] * factors[1] * factors[2]
    for source in range(total):
        place = source // inner % factors[axis]
        pairs.append((source, source + ((place + step) % factors[axis] - place) * inner))
    return pairs


def own_place(factors, axis):
    inner = 1
    for size in factors[axis + 1 :]:
        inner *= size
    return lax.axis_index("ep") // inner % factors[axis]


def reduce_stage(parts, factors, axis, dim):
    size = factors[axis]
    place = own_place(factors, axis)
    total = lax.dynamic_index_in_dim(parts, place, dim, keepdims=True).astype(jnp.float32)
    for step in range(1, size):
        sent = lax.dynamic_index_in_dim(parts, (place + step) % size, dim, keepdims=True)
        total = total + lax.ppermute(
            sent.astype(jnp.bfloat16), "ep", shift_pairs(factors, axis, step)
        ).astype(jnp.float32)
    return total


def staged_reduce_scatter(partial, factors, order):
    rows = partial.shape[0] // (factors[0] * factors[1] * factors[2])
    parts = partial.reshape(*factors, rows, partial.shape[1])
    for axis in order:
        parts = reduce_stage(parts, factors, axis, axis)
    return parts.reshape(rows, partial.shape[1])


def swap_cores(values_in):
    return lax.ppermute(values_in, "tp", [(0, 1), (1, 0)])


def body(
    tokens,
    mix_gain,
    w_query,
    w_key,
    w_value,
    w_outgate,
    w_igate,
    w_fgate,
    igate_bias,
    fgate_bias,
    head_gain,
    w_out,
    state_matrix,
    state_norm,
    state_max,
    ffn_gain,
    w_expert_gate,
    w_expert_up,
    w_expert_down,
    routes,
    route_weights,
):
    seq_rows, width = tokens.shape
    ep_count = lax.axis_size("ep")
    factors = torus_factors(ep_count)
    w_out_full = lax.all_gather(w_out, "ep", axis=1, tiled=True)
    local_experts = w_expert_gate.shape[0]
    expert_total = local_experts * ep_count
    top_count = routes.shape[1]
    capacity = max(2, 2 * seq_rows * top_count // expert_total)
    core_slots = -(-((capacity + 1) // 2) // 8) * 8
    core = lax.axis_index("tp")
    flat_routes = routes.reshape(-1)
    onehot = (flat_routes[:, None] == jnp.arange(expert_total, dtype=jnp.int32)[None, :]).astype(
        jnp.int32
    )
    earlier = jnp.cumsum(onehot, axis=0, dtype=jnp.int32) - onehot
    slots = jnp.sum(onehot * earlier, axis=1, dtype=jnp.int32)
    targets = jnp.where(slots % 2 == core, flat_routes * core_slots + slots // 2, -1)
    places = jnp.arange(expert_total * core_slots, dtype=jnp.int32)
    hits = (targets[:, None] == places[None, :]).reshape(seq_rows, top_count, -1)
    token_hits = jnp.any(hits, axis=1).astype(jnp.bfloat16)
    weight_hits = jnp.sum(jnp.where(hits, route_weights[:, :, None], 0.0), axis=1)
    normed = rms_scale(tokens, mix_gain).astype(jnp.bfloat16)
    spread = lax.all_to_all(normed, "ep", split_axis=1, concat_axis=0, tiled=True)
    first_list = (w_query, w_key)
    second_list = (w_value, w_outgate, w_igate, w_fgate)
    first = staged_reduce_scatter(
        jnp.dot(
            spread, jnp.concatenate(first_list, axis=1), preferred_element_type=jnp.float32
        ).astype(jnp.bfloat16),
        factors,
        (2, 1, 0),
    )
    second = staged_reduce_scatter(
        jnp.dot(
            spread, jnp.concatenate(second_list, axis=1), preferred_element_type=jnp.float32
        ).astype(jnp.bfloat16),
        factors,
        (1, 2, 0),
    )
    head_width = w_query.shape[1]
    head_count = w_igate.shape[1]
    query = first[:, :head_width].astype(jnp.bfloat16)
    key_row = first[:, head_width:].astype(jnp.bfloat16)
    value_row = second[:, :head_width].astype(jnp.bfloat16)
    outgate = second[:, head_width : 2 * head_width].astype(jnp.bfloat16)
    input_pre = second[:, 2 * head_width : 2 * head_width + head_count] + igate_bias
    forget_pre = second[:, 2 * head_width + head_count :] + fgate_bias
    cell_out, new_matrix, new_norm, new_max = memory_cell(
        query,
        key_row,
        value_row,
        outgate,
        input_pre,
        forget_pre,
        head_gain,
        state_matrix,
        state_norm,
        state_max,
    )
    partial_out = jnp.dot(cell_out, w_out_full, preferred_element_type=jnp.float32).astype(
        jnp.bfloat16
    )
    attended = partial_out.astype(jnp.float32) + swap_cores(partial_out).astype(jnp.float32)
    resid = (tokens.astype(jnp.float32) + attended).astype(jnp.bfloat16)
    normed_two = rms_scale(resid, ffn_gain).astype(jnp.bfloat16)
    outgoing = lax.dot_general(
        token_hits, normed_two, (((0,), (0,)), ((), ())), preferred_element_type=jnp.float32
    ).astype(jnp.bfloat16)
    outgoing = outgoing.reshape(expert_total, core_slots, width)
    received = lax.all_to_all(outgoing, "ep", split_axis=0, concat_axis=0, tiled=True)
    other = swap_cores(received)

    def grouped(rows):
        rows = rows.reshape(ep_count, local_experts, core_slots, width)
        return jnp.swapaxes(rows, 0, 1).reshape(local_experts, ep_count * core_slots, width)

    regrouped = jnp.concatenate([grouped(received), grouped(other)], axis=1)
    gate_pre = jnp.einsum(
        "xcd,xdf->xcf", regrouped, w_expert_gate, preferred_element_type=jnp.float32
    )
    up_pre = jnp.einsum("xcd,xdf->xcf", regrouped, w_expert_up, preferred_element_type=jnp.float32)
    hidden = (jax.nn.silu(gate_pre) * up_pre).astype(jnp.bfloat16)
    partial_down = jnp.einsum(
        "xcf,xfd->xcd", hidden, w_expert_down, preferred_element_type=jnp.float32
    ).astype(jnp.bfloat16)
    half = ep_count * core_slots
    expert_sum = (
        partial_down[:, :half].astype(jnp.float32)
        + swap_cores(partial_down[:, half:]).astype(jnp.float32)
    ).astype(jnp.bfloat16)
    finished = jnp.swapaxes(
        expert_sum.reshape(local_experts, ep_count, core_slots, width), 0, 1
    ).reshape(ep_count * local_experts, core_slots, width)
    returned = lax.all_to_all(finished, "ep", split_axis=0, concat_axis=0, tiled=True)
    returned = returned.reshape(expert_total * core_slots, width)
    weight_high = weight_hits.astype(jnp.bfloat16)
    weight_rest = weight_hits - weight_high.astype(jnp.float32)
    weight_low = weight_rest.astype(jnp.bfloat16)
    weighted = jnp.dot(weight_high, returned, preferred_element_type=jnp.float32) + jnp.dot(
        weight_low, returned, preferred_element_type=jnp.float32
    )
    weighted = weighted + swap_cores(weighted)
    mixed = (resid.astype(jnp.float32) + weighted).astype(jnp.bfloat16)
    return (mixed, new_matrix, new_norm, new_max)


def solution(mesh):
    placed = (
        P("ep", None),
        P(),
        P("ep", "tp"),
        P("ep", "tp"),
        P("ep", "tp"),
        P("ep", "tp"),
        P("ep", "tp"),
        P("ep", "tp"),
        P("tp"),
        P("tp"),
        P("tp"),
        P("tp", "ep"),
        P("ep", "tp", None, None),
        P("ep", "tp", None),
        P("ep", "tp"),
        P(),
        P("ep", None, "tp"),
        P("ep", None, "tp"),
        P("ep", "tp", None),
        P("ep", None),
        P("ep", None),
    )
    return jax.shard_map(
        body,
        mesh=mesh,
        in_specs=placed,
        out_specs=(P("ep", None), P("ep", "tp", None, None), P("ep", "tp", None), P("ep", "tp")),
        check_vma=False,
    )
```

profile of v0, /device:TPU:0, one launch (start us, length us, event | category | flops | bytes accessed | tf_op | source)
XLA Modules:
  0.0 143.0 jit_solution(14538455272105460633)
XLA Ops:
  7.9 1.2 fusion.29
  9.1 1.7 %copy_bitcast_fusion = bf16[32,16,128]{2,0,1:T(8,128)(2,1)} fusion(bf16[32,2048]{1,0:T(8,128)(2,1)} %param.21, f32[2048]{0:T(1024)} %param.22, f32[32]{0:T(128)S(1)} %add_rsqrt_fusion.2), kind=kLoop, calls=%fused_computation.56 | loop fusion | flops 262144 | bytes 270464 | tf_op jit(solution)/shard_map/all_to_all | solution.py:151
  10.8 8.3 %all-to-all-start = ((bf16[32,16,128]{2,0,1:T(8,128)(2,1)}), bf16[32,16,128]{2,0,1:T(8,128)(2,1)S(1)}, u32[]{:S(2)}, u32[]{:S(2)}) async-start(bf16[32,16,128]{2,0,1:T(8,128)(2,1)} %copy_bitcast_fusion), calls=%async_computation | async-start | bytes 262144 | tf_op jit(solution)/shard_map/all_to_all | solution.py:151
  19.2 1.4 copy.61
  24.3 2.6 %all-to-all-done = bf16[32,16,128]{2,0,1:T(8,128)(2,1)S(1)} async-done(((bf16[32,16,128]{2,0,1:T(8,128)(2,1)}), bf16[32,16,128]{2,0,1:T(8,128)(2,1)S(1)}, u32[]{:S(2)}, u32[]{:S(2)}) %all-to-all-start) | async-done | bytes 131104 | tf_op jit(solution)/shard_map/all_to_all | solution.py:151
  26.9 1.2 convolution_convert_fusion.3
  28.9 1.1 collective-permute-start.5
  30.0 2.0 %convolution_convert_fusion.2 = bf16[512,520]{0,1:T(8,128)(2,1)} fusion(bf16[512,128]{1,0:T(8,128)(2,1)S(1)} %bitcast.61, bf16[128,4]{1,0:T(8,128)(2,1)S(1)} %copy.59, bf16[128,4]{1,0:T(8,128)(2,1)S(1)} %copy.58, bf16[128,256]{1,0:T(8,128)(2,1)} %param.26, bf16[128,256]{1,0:T(8,128)(2,1)} %param.25), kind=kOutput, calls=%fused_computation.14 | convolution fusion | flops 68956160 | bytes 796672 | tf_op jit(solution)/shard_map/dot_general | solution.py:162
  32.0 1.3 copy.60
  33.6 2.2 %collective-permute-done.5 = bf16[4,2,1,32,512]{4,3,2,1,0:T(8,128)(2,1)} collective-permute-done((bf16[4,2,1,32,512]{4,3,2,1,0:T(8,128)(2,1)}, bf16[4,2,1,32,512]{4,3,2,1,0:T(8,128)(2,1)}, u32[]{:S(2)}, u32[]{:S(2)}) %collective-permute-start.5) | collective-permute-done | bytes 262176 | tf_op jit(solution)/shard_map/ppermute | solution.py:88
  35.8 1.1 convert_add_fusion.1
  38.0 6.3 %collective-permute-done = bf16[4,1,2,32,520]{4,3,2,1,0:T(8,128)(2,1)S(1)} collective-permute-done((bf16[4,1,2,32,520]{4,3,2,1,0:T(8,128)(2,1)S(1)}, bf16[4,1,2,32,520]{4,3,2,1,0:T(8,128)(2,1)S(1)}, u32[]{:S(2)}, u32[]{:S(2)}) %collective-permute-start) | collective-permute-done | bytes 266272 | tf_op jit(solution)/shard_map/ppermute | solution.py:88
  46.1 3.5 %collective-permute-start.9 = (bf16[1,1,1,32,512]{4,3,2,1,0:T(8,128)(2,1)S(1)}, bf16[1,1,1,32,512]{4,3,2,1,0:T(8,128)(2,1)S(1)}, u32[]{:S(2)}, u32[]{:S(2)}) collective-permute-start(bf16[1,1,1,32,512]{4,3,2,1,0:T(8,128)(2,1)S(1)} %get-tuple-element.33), channel_id=1, source_target_pairs={{0,24},{2,26},{4,28},{6,30},{8,0},{10,2},{12,4},{14,6},{16,8},{18,... | collective-permute-start | bytes 98312 | tf_op jit(solution)/shard_map/ppermute | solution.py:88
  51.0 3.3 %collective-permute-start.4 = (bf16[1,1,1,32,520]{4,3,2,1,0:T(8,128)(2,1)}, bf16[1,1,1,32,520]{4,3,2,1,0:T(8,128)(2,1)S(1)}, u32[]{:S(2)}, u32[]{:S(2)}) collective-permute-start(bf16[1,1,1,32,520]{4,3,2,1,0:T(8,128)(2,1)} %get-tuple-element.30), channel_id=1, source_target_pairs={{0,24},{2,26},{4,28},{6,30},{8,0},{10,2},{12,4},{14,6},{16,8},{18,... | collective-permute-start | bytes 99848 | tf_op jit(solution)/shard_map/ppermute | solution.py:88
  55.5 1.7 %collective-permute-done.2 = bf16[1,1,1,32,520]{4,3,2,1,0:T(8,128)(2,1)S(1)} collective-permute-done((bf16[1,1,1,32,520]{4,3,2,1,0:T(8,128)(2,1)}, bf16[1,1,1,32,520]{4,3,2,1,0:T(8,128)(2,1)S(1)}, u32[]{:S(2)}, u32[]{:S(2)}) %collective-permute-start.2) | collective-permute-done | bytes 33312 | tf_op jit(solution)/shard_map/ppermute | solution.py:88
  57.9 2.1 %collective-permute-done.3 = bf16[1,1,1,32,520]{4,3,2,1,0:T(8,128)(2,1)} collective-permute-done((bf16[1,1,1,32,520]{4,3,2,1,0:T(8,128)(2,1)S(1)}, bf16[1,1,1,32,520]{4,3,2,1,0:T(8,128)(2,1)}, u32[]{:S(2)}, u32[]{:S(2)}) %collective-permute-start.3) | collective-permute-done | bytes 33312 | tf_op jit(solution)/shard_map/ppermute | solution.py:88
  62.6 1.6 %multiply_reduce_fusion.2 = (f32[32,4]{1,0:T(8,128)S(1)}, f32[32,4,64]{2,1,0:T(4,128)}, f32[32,4,64]{2,1,0:T(4,128)S(1)}, f32[32,4,64]{2,1,0:T(4,128)S(1)}) fusion(f32[32,4,64]{2,1,0:T(4,128)S(1)} %reshape.188, f32[32,4,64]{2,1,0:T(4,128)S(1)} %reshape.187, f32[32,4]{1,0:T(8,128)S(1)} %get-tuple-element.22, f32[32,4,64]{2,1,0:T(4,128)} %param.34, ...), kind=kLoop, calls=%fused_computation.67 | loop fusion | flops 57216 | bytes 231424 | tf_op jit(solution)/shard_map/reduce_sum | solution.py:43
  64.3 6.3 %multiply_reduce_fusion = (f32[32,4,64]{2,1,0:T(4,128)S(1)}, f32[32,4,64,64]{3,2,1,0:T(8,128)}) fusion(f32[32,4,64]{2,1,0:T(4,128)S(1)} %reshape.188, f32[32,4,64]{2,1,0:T(4,128)S(1)} %get-tuple-element.35, f32[32,4,64]{2,1,0:T(4,128)S(1)} %get-tuple-element.38, f32[32,4,64,64]{3,2,1,0:T(8,128)} %param.33, f32[32,4]{1,0:T(8,128)S(1)} %subtract_exponential_fusion.1), kind=kLoop, calls=%fused_computation | loop fusion | flops 2613248 | bytes 4325888 | tf_op jit(solution)/shard_map/reduce_sum | solution.py:42
  71.3 1.6 %convolution_convert_fusion.1 = bf16[32,2048]{1,0:T(8,128)(2,1)S(1)} fusion(bf16[256,2048]{1,0:T(8,128)(2,1)} %all-gather.2.cloned.1.call-done, f32[32,256]{1,0:T(8,128)S(1)} %mul.194, bf16[32,520]{1,0:T(8,128)(2,1)S(1)} %get-tuple-element.27, f32[256]{0:T(256)S(1)} %copy-done.8), kind=kOutput, calls=%fused_computation.13 | convolution fusion | flops 33677312 | bytes 1229824 | tf_op jit(solution)/shard_map/dot_general | solution.py:188
  73.1 1.2 collective-permute-done.10
  74.9 19.9 %all_to_all.29 = bf16[16,8,2048]{2,1,0:T(8,128)(2,1)S(1)} all-to-all(bf16[16,8,2048]{2,1,0:T(8,128)(2,1)S(1)} %fusion.12), channel_id=1, replica_groups=mesh['ep'=16,'tp'=2] {'ep'}, dimensions={0} | all-to-all | bytes 1048576 | tf_op jit(solution)/shard_map/all_to_all | solution.py:198
  94.8 1.9 %collective-permute-done.11 = bf16[16,8,2048]{2,1,0:T(8,128)(2,1)S(1)} collective-permute-done((bf16[16,8,2048]{2,1,0:T(8,128)(2,1)S(1)}, bf16[16,8,2048]{2,1,0:T(8,128)(2,1)S(1)}, u32[]{:S(2)}, u32[]{:S(2)}) %collective-permute-start.11) | collective-permute-done | bytes 524320 | tf_op jit(solution)/shard_map/ppermute | solution.py:103
  97.5 1.8 %fusion.4 = f32[256,704]{0,1:T(8,128)} fusion(bf16[1,2048,704]{1,2,0:T(8,128)(2,1)S(1)} %copy-done.9, bf16[1,128,2048]{2,1,0:T(8,128)(2,1)S(1)} %bitcast.64, bf16[1,128,2048]{2,1,0:T(8,128)(2,1)S(1)} %bitcast.62), kind=kOutput, calls=%fused_computation.6 | convolution fusion | flops 740294656 | bytes 4653056 | tf_op jit(solution)/shard_map/xcd,xdf->xcf/dot_general | solution.py:206
  99.4 6.4 %fusion.9 = bf16[1,256,2048]{2,1,0:T(8,128)(2,1)} fusion(bf16[1,704,2048]{2,1,0:T(8,128)(2,1)S(1)} %copy-done, bf16[1,2048,704]{1,2,0:T(8,128)(2,1)} %param.38, f32[256,704]{0,1:T(8,128)} %fusion.4, bf16[1,128,2048]{2,1,0:T(8,128)(2,1)} %bitcast.65, bf16[1,128,2048]{2,1,0:T(8,128)(2,1)S(1)} %bitcast.63), kind=kOutput, calls=%fused_computation.9 | convolution fusion | flops 1480097792 | bytes 8585216 | tf_op jit(solution)/shard_map/xcf,xfd->xcd/dot_general | solution.py:211
  107.0 1.8 %collective-permute-done.12 = bf16[1,128,2048]{2,1,0:T(8,128)(2,1)S(1)} collective-permute-done((bf16[1,128,2048]{2,1,0:T(8,128)(2,1)S(1)}, bf16[1,128,2048]{2,1,0:T(8,128)(2,1)S(1)}, u32[]{:S(2)}, u32[]{:S(2)}) %collective-permute-start.12) | collective-permute-done | bytes 524320 | tf_op jit(solution)/shard_map/ppermute | solution.py:103
  108.8 2.0 %fusion.24 = bf16[16,8,2048]{2,1,0:T(8,128)(2,1)} fusion(bf16[1,128,2048]{2,1,0:T(8,128)(2,1)S(1)} %collective-permute-done.12, bf16[1,256,2048]{2,1,0:T(8,128)(2,1)} %fusion.9), kind=kLoop, calls=%fused_computation.24 | loop fusion | flops 1048576 | bytes 1572864 | tf_op jit(solution)/shard_map/reshape;transpose;reshape | solution.py:221
  110.8 3.9 %all-to-all-start.2 = ((bf16[16,8,2048]{2,1,0:T(8,128)(2,1)}), bf16[16,8,2048]{2,1,0:T(8,128)(2,1)S(1)}, u32[]{:S(2)}, u32[]{:S(2)}) async-start(bf16[16,8,2048]{2,1,0:T(8,128)(2,1)} %fusion.24), calls=%async_computation.2 | async-start | bytes 1048576 | tf_op jit(solution)/shard_map/all_to_all | solution.py:222
  114.8 1.4 select_reduce_fusion
  116.2 14.0 %all-to-all-done.2 = bf16[16,8,2048]{2,1,0:T(8,128)(2,1)S(1)} async-done(((bf16[16,8,2048]{2,1,0:T(8,128)(2,1)}), bf16[16,8,2048]{2,1,0:T(8,128)(2,1)S(1)}, u32[]{:S(2)}, u32[]{:S(2)}) %all-to-all-start.2) | async-done | bytes 524320 | tf_op jit(solution)/shard_map/all_to_all | solution.py:222
  131.1 1.7 %convolution_add_fusion = f32[32,2048]{1,0:T(8,128)} fusion(f32[32,2048]{1,0:T(8,128)S(1)} %fusion.26, bf16[16,8,2048]{2,1,0:T(8,128)(2,1)S(1)} %all-to-all-done.2, f32[32,128]{1,0:T(8,128)} %select_reduce_fusion), kind=kOutput, calls=%fused_computation.12 | convolution fusion | flops 16859136 | bytes 1064960 | tf_op jit(solution)/shard_map/dot_general | solution.py:227
  133.4 1.1 collective-permute-done.13
  134.5 1.6 %fusion.36 = bf16[32,2048]{1,0:T(8,128)(2,1)} fusion(bf16[32,2048]{1,0:T(8,128)(2,1)S(1)} %get-tuple-element.17, f32[32,2048]{1,0:T(8,128)} %convolution_add_fusion, f32[32,2048]{1,0:T(8,128)S(1)} %collective-permute-done.13), kind=kLoop, calls=%fused_computation.45 | loop fusion | flops 262144 | bytes 786432 | tf_op jit(solution)/shard_map/convert_element_type | solution.py:231
  (85 shorter events, 19.1 us)
Async XLA Ops:
  7.2 92.2 %copy-start = (bf16[1,704,2048]{2,1,0:T(8,128)(2,1)S(1)}, bf16[1,704,2048]{2,1,0:T(8,128)(2,1)}, u32[]{:S(2)}) copy-start(bf16[1,704,2048]{2,1,0:T(8,128)(2,1)} %param.39) | copy-start | bytes 8650756
  7.2 64.1 %all-gather.2.cloned.1.call-start = ((), (), s32[]{:S(2)}) async-start(), calls=%async_computation.3 | async-start | bytes 1114112 | tf_op jit(solution)/shard_map/all_gather | solution.py:132
  10.8 16.1 %all-to-all-start = ((bf16[32,16,128]{2,0,1:T(8,128)(2,1)}), bf16[32,16,128]{2,0,1:T(8,128)(2,1)S(1)}, u32[]{:S(2)}, u32[]{:S(2)}) async-start(bf16[32,16,128]{2,0,1:T(8,128)(2,1)} %copy_bitcast_fusion), calls=%async_computation | async-start | bytes 262144 | tf_op jit(solution)/shard_map/all_to_all | solution.py:151
  28.1 1.9 %copy-start.1 = (bf16[512,512]{1,0:T(8,128)(2,1)}, bf16[512,512]{1,0:T(8,128)(2,1)S(1)}, u32[]{:S(2)}) copy-start(bf16[512,512]{1,0:T(8,128)(2,1)S(1)} %convolution_convert_fusion.3) | copy-start | bytes 1572868
  28.9 6.9 %collective-permute-start.5 = (bf16[4,2,1,32,512]{4,3,2,1,0:T(8,128)(2,1)}, bf16[4,2,1,32,512]{4,3,2,1,0:T(8,128)(2,1)}, u32[]{:S(2)}, u32[]{:S(2)}) collective-permute-start(bf16[4,2,1,32,512]{4,3,2,1,0:T(8,128)(2,1)} %constant_dynamic-slice_fusion), channel_id=1, source_target_pairs={{0,2},{2,0},{4,6},{6,4},{8,10},{10,8},{12,14},{14,12},{16,18},{18,... | collective-permute-start | bytes 786440 | tf_op jit(solution)/shard_map/ppermute | solution.py:88
  33.4 10.9 %collective-permute-start = (bf16[4,1,2,32,520]{4,3,2,1,0:T(8,128)(2,1)S(1)}, bf16[4,1,2,32,520]{4,3,2,1,0:T(8,128)(2,1)S(1)}, u32[]{:S(2)}, u32[]{:S(2)}) collective-permute-start(bf16[4,1,2,32,520]{4,3,2,1,0:T(8,128)(2,1)S(1)} %constant_dynamic-slice_fusion.1), channel_id=1, source_target_pairs={{0,4},{2,6},{4,0},{6,2},{8,12},{10,14},{12,8},{14,10},{16,20},{18,... | collective-permute-start | bytes 798728 | tf_op jit(solution)/shard_map/ppermute | solution.py:88
  36.9 8.7 %collective-permute-start.6 = (bf16[4,1,1,32,512]{4,3,2,1,0:T(8,128)(2,1)S(1)}, bf16[4,1,1,32,512]{4,3,2,1,0:T(8,128)(2,1)S(1)}, u32[]{:S(2)}, u32[]{:S(2)}) collective-permute-start(bf16[4,1,1,32,512]{4,3,2,1,0:T(8,128)(2,1)S(1)} %dynamic-slice_convert_fusion.1), channel_id=1, source_target_pairs={{0,4},{2,6},{4,0},{6,2},{8,12},{10,14},{12,8},{14,10},{16,20},{18,... | collective-permute-start | bytes 393224 | tf_op jit(solution)/shard_map/ppermute | solution.py:88
  44.4 5.4 %collective-permute-start.1 = (bf16[4,1,1,32,520]{4,3,2,1,0:T(8,128)(2,1)S(1)}, bf16[4,1,1,32,520]{4,3,2,1,0:T(8,128)(2,1)S(1)}, u32[]{:S(2)}, u32[]{:S(2)}) collective-permute-start(bf16[4,1,1,32,520]{4,3,2,1,0:T(8,128)(2,1)S(1)} %dynamic-slice_convert_fusion), channel_id=1, source_target_pairs={{0,2},{2,0},{4,6},{6,4},{8,10},{10,8},{12,14},{14,12},{16,18},{18,... | collective-permute-start | bytes 399368 | tf_op jit(solution)/shard_map/ppermute | solution.py:88
  45.8 8.6 %collective-permute-start.7 = (bf16[1,1,1,32,512]{4,3,2,1,0:T(8,128)(2,1)S(1)}, bf16[1,1,1,32,512]{4,3,2,1,0:T(8,128)(2,1)S(1)}, u32[]{:S(2)}, u32[]{:S(2)}) collective-permute-start(bf16[1,1,1,32,512]{4,3,2,1,0:T(8,128)(2,1)S(1)} %get-tuple-element.32), channel_id=1, source_target_pairs={{0,8},{2,10},{4,12},{6,14},{8,16},{10,18},{12,20},{14,22},{16,24},... | collective-permute-start | bytes 98312 | tf_op jit(solution)/shard_map/ppermute | solution.py:88
  46.1 9.1 %collective-permute-start.9 = (bf16[1,1,1,32,512]{4,3,2,1,0:T(8,128)(2,1)S(1)}, bf16[1,1,1,32,512]{4,3,2,1,0:T(8,128)(2,1)S(1)}, u32[]{:S(2)}, u32[]{:S(2)}) collective-permute-start(bf16[1,1,1,32,512]{4,3,2,1,0:T(8,128)(2,1)S(1)} %get-tuple-element.33), channel_id=1, source_target_pairs={{0,24},{2,26},{4,28},{6,30},{8,0},{10,2},{12,4},{14,6},{16,8},{18,... | collective-permute-start | bytes 98312 | tf_op jit(solution)/shard_map/ppermute | solution.py:88
  49.6 5.7 %collective-permute-start.8 = (bf16[1,1,1,32,512]{4,3,2,1,0:T(8,128)(2,1)S(1)}, bf16[1,1,1,32,512]{4,3,2,1,0:T(8,128)(2,1)S(1)}, u32[]{:S(2)}, u32[]{:S(2)}) collective-permute-start(bf16[1,1,1,32,512]{4,3,2,1,0:T(8,128)(2,1)S(1)} %get-tuple-element.34), channel_id=1, source_target_pairs={{0,16},{2,18},{4,20},{6,22},{8,24},{10,26},{12,28},{14,30},{16,0},... | collective-permute-start | bytes 98312 | tf_op jit(solution)/shard_map/ppermute | solution.py:88
  50.5 6.8 %collective-permute-start.2 = (bf16[1,1,1,32,520]{4,3,2,1,0:T(8,128)(2,1)}, bf16[1,1,1,32,520]{4,3,2,1,0:T(8,128)(2,1)S(1)}, u32[]{:S(2)}, u32[]{:S(2)}) collective-permute-start(bf16[1,1,1,32,520]{4,3,2,1,0:T(8,128)(2,1)} %get-tuple-element.29), channel_id=1, source_target_pairs={{0,8},{2,10},{4,12},{6,14},{8,16},{10,18},{12,20},{14,22},{16,24},... | collective-permute-start | bytes 99848 | tf_op jit(solution)/shard_map/ppermute | solution.py:88
  51.0 6.3 %collective-permute-start.4 = (bf16[1,1,1,32,520]{4,3,2,1,0:T(8,128)(2,1)}, bf16[1,1,1,32,520]{4,3,2,1,0:T(8,128)(2,1)S(1)}, u32[]{:S(2)}, u32[]{:S(2)}) collective-permute-start(bf16[1,1,1,32,520]{4,3,2,1,0:T(8,128)(2,1)} %get-tuple-element.30), channel_id=1, source_target_pairs={{0,24},{2,26},{4,28},{6,30},{8,0},{10,2},{12,4},{14,6},{16,8},{18,... | collective-permute-start | bytes 99848 | tf_op jit(solution)/shard_map/ppermute | solution.py:88
  54.3 5.7 %collective-permute-start.3 = (bf16[1,1,1,32,520]{4,3,2,1,0:T(8,128)(2,1)S(1)}, bf16[1,1,1,32,520]{4,3,2,1,0:T(8,128)(2,1)}, u32[]{:S(2)}, u32[]{:S(2)}) collective-permute-start(bf16[1,1,1,32,520]{4,3,2,1,0:T(8,128)(2,1)S(1)} %get-tuple-element.31), channel_id=1, source_target_pairs={{0,16},{2,18},{4,20},{6,22},{8,24},{10,26},{12,28},{14,30},{16,0},... | collective-permute-start | bytes 99848 | tf_op jit(solution)/shard_map/ppermute | solution.py:88
  57.3 0.6 copy-start.3
  64.2 7.1 %copy-start.8 = (f32[256]{0:T(256)S(1)}, f32[256]{0:T(256)}, u32[]{:S(2)}) copy-start(f32[256]{0:T(256)} %param.31) | copy-start | bytes 3076
  64.2 8.8 %copy-start.6 = (s32[32,3]{0,1:T(4,128)S(1)}, s32[32,3]{0,1:T(4,128)}, u32[]{:S(2)}) copy-start(s32[32,3]{0,1:T(4,128)} %param.40) | copy-start | bytes 1156
  64.2 8.7 %copy-start.7 = (s32[32,3]{0,1:T(4,128)S(1)}, s32[32,3]{0,1:T(4,128)}, u32[]{:S(2)}) copy-start(s32[32,3]{0,1:T(4,128)} %copy.63) | copy-start | bytes 1156
  64.3 10.1 %copy-start.2 = (bf16[32,2048]{1,0:T(8,128)(2,1)S(1)}, bf16[32,2048]{1,0:T(8,128)(2,1)}, u32[]{:S(2)}) copy-start(bf16[32,2048]{1,0:T(8,128)(2,1)} %param.21) | copy-start | bytes 393220
  64.3 10.2 %copy-start.5 = (f32[2048]{0:T(1024)S(1)}, f32[2048]{0:T(1024)}, u32[]{:S(2)}) copy-start(f32[2048]{0:T(1024)} %param.36) | copy-start | bytes 24580
  71.3 26.3 %copy-start.9 = (bf16[1,2048,704]{1,2,0:T(8,128)(2,1)S(1)}, bf16[1,2048,704]{1,2,0:T(8,128)(2,1)}, u32[]{:S(2)}) copy-start(bf16[1,2048,704]{1,2,0:T(8,128)(2,1)} %param.37) | copy-start | bytes 8650756
  72.9 1.4 collective-permute-start.10
  73.0 1.5 %copy-start.4 = (s32[32,3]{0,1:T(4,128)}, s32[32,3]{0,1:T(4,128)S(1)}, u32[]{:S(2)}) copy-start(s32[32,3]{0,1:T(4,128)S(1)} %fusion.65) | copy-start | bytes 1156
  94.8 1.9 %collective-permute-start.11 = (bf16[16,8,2048]{2,1,0:T(8,128)(2,1)S(1)}, bf16[16,8,2048]{2,1,0:T(8,128)(2,1)S(1)}, u32[]{:S(2)}, u32[]{:S(2)}) collective-permute-start(bf16[16,8,2048]{2,1,0:T(8,128)(2,1)S(1)} %all_to_all.29), channel_id=1, source_target_pairs={{0,1},{1,0},{2,3},{3,2},{4,5},{5,4},{6,7},{7,6},{8,9},{9,8},{10,11... | collective-permute-start | bytes 1572872 | tf_op jit(solution)/shard_map/ppermute | solution.py:103
  96.7 0.8 copy-start.10
  106.9 2.0 %collective-permute-start.12 = (bf16[1,128,2048]{2,1,0:T(8,128)(2,1)S(1)}, bf16[1,128,2048]{2,1,0:T(8,128)(2,1)S(1)}, u32[]{:S(2)}, u32[]{:S(2)}) collective-permute-start(bf16[1,128,2048]{2,1,0:T(8,128)(2,1)S(1)} %slice.43), channel_id=1, source_target_pairs={{0,1},{1,0},{2,3},{3,2},{4,5},{5,4},{6,7},{7,6},{8,9},{9,8},{10,11... | collective-permute-start | bytes 1572872 | tf_op jit(solution)/shard_map/ppermute | solution.py:103
  110.8 19.3 %all-to-all-start.2 = ((bf16[16,8,2048]{2,1,0:T(8,128)(2,1)}), bf16[16,8,2048]{2,1,0:T(8,128)(2,1)S(1)}, u32[]{:S(2)}, u32[]{:S(2)}) async-start(bf16[16,8,2048]{2,1,0:T(8,128)(2,1)} %fusion.24), calls=%async_computation.2 | async-start | bytes 1048576 | tf_op jit(solution)/shard_map/all_to_all | solution.py:222
  132.8 1.7 %collective-permute-start.13 = (f32[32,2048]{1,0:T(8,128)}, f32[32,2048]{1,0:T(8,128)S(1)}, u32[]{:S(2)}, u32[]{:S(2)}) collective-permute-start(f32[32,2048]{1,0:T(8,128)} %convolution_add_fusion), channel_id=1, source_target_pairs={{0,1},{1,0},{2,3},{3,2},{4,5},{5,4},{6,7},{7,6},{8,9},{9,8},{10,11... | collective-permute-start | bytes 786440 | tf_op jit(solution)/shard_map/ppermute | solution.py:103
Sparse Core Ops, SparseCore 0:
  10.7 57.9 all-gather.1
where the time goes:
time: 144 us; the launch traced here: 143 us
  waiting for transfers between devices  36.3 us (25%)
  starting transfers between devices  24.3 us (17%)
  other arithmetic  20.7 us (14%)
  blocking collectives  19.9 us (14%)
  matrix products  16 us (11%)
  between operations  14.5 us (10%)
  local copies, waits for them, and re-layouts  11.1 us (8%)
    all_to_all x1, blocking collectives, body(): lax.all_to_all(outgoing, 'ep', split_axis=0, concat_axis=0, tiled=True)  19.9 us
    all_to_all x1, waiting for transfers between devices, body(): lax.all_to_all(finished, 'ep', split_axis=0, concat_axis=0, tiled=True)  14 us
    ppermute x10, waiting for transfers between devices, reduce_stage(): lax.ppermute(sent.astype(jnp.bfloat16), 'ep', shift_pairs(factors, axis,...  13.1 us
    ppermute x10, starting transfers between devices, reduce_stage(): lax.ppermute(sent.astype(jnp.bfloat16), 'ep', shift_pairs(factors, axis,...  11.8 us
    all_to_all x1, starting transfers between devices, body(): lax.all_to_all(normed, 'ep', split_axis=1, concat_axis=0, tiled=True)  8.34 us
    dot_general x1, matrix products, body(): jnp.einsum('xcf,xfd->xcd', hidden, w_expert_down, preferred_element_type=...  6.4 us
    reduce_sum x1, other arithmetic, memory_cell(): numerator = jnp.sum(new_matrix * query_heads[:, :, None, :], axis=-1)  6.35 us
    ppermute x4, waiting for transfers between devices, swap_cores(): return lax.ppermute(values_in, 'tp', [(0, 1), (1, 0)])  5.98 us
  transfers between devices with their start and end apart: 17, of which 12 were waited for; matrix products, arithmetic and copies ran while one was open for 20% of the time, Pallas kernels for 0%

commit v1 on v0

--- a/solution.py
+++ b/solution.py
@@ -148,7 +148,12 @@
     token_hits = jnp.any(hits, axis=1).astype(jnp.bfloat16)
     weight_hits = jnp.sum(jnp.where(hits, route_weights[:, :, None], 0.0), axis=1)
     normed = rms_scale(tokens, mix_gain).astype(jnp.bfloat16)
-    spread = lax.all_to_all(normed, "ep", split_axis=1, concat_axis=0, tiled=True)
+    spread = jnp.concatenate(
+        lax.all_to_all(
+            jnp.stack(jnp.split(normed, lax.axis_size("ep"), axis=1), axis=0), "ep", 0, 0
+        ),
+        axis=0,
+    )
     first_list = (w_query, w_key)
     second_list = (w_value, w_outgate, w_igate, w_fgate)
     first = staged_reduce_scatter(

time: 144 us -> 153 us (1.062)
  local copies, waits for them, and re-layouts: 11.1 us -> 20.8 us
  waiting for transfers between devices: 36.3 us -> 38.3 us
    unnamed x27 -> x46, local copies, waits for them, and re-layouts: 5.88 us -> 14.9 us
    ppermute x10, waiting for transfers between devices: 13.1 us -> 15.1 us  [reduce_stage(): lax.ppermute(sent.astype(jnp.bfloat16), 'ep', shift_pairs(factors, axis,...]
    all_to_all x1 -> x0, other arithmetic: 1.67 us -> none  [body(): lax.all_to_all(normed, 'ep', split_axis=1, concat_axis=0, tiled=True)]
  transfers between devices with their start and end apart: 17 -> 17, of which waited for: 12 -> 12; matrix products, arithmetic and copies ran while one was open for 20% -> 24% of each run, Pallas kernels for 0% -> 0%
where the time goes in v1:
time: 153 us; the launch traced here: 151 us
  waiting for transfers between devices  38.3 us (25%)
  starting transfers between devices  23.4 us (15%)
  local copies, waits for them, and re-layouts  20.8 us (14%)
  other arithmetic  20.1 us (13%)
  blocking collectives  19.2 us (13%)
  matrix products  15.2 us (10%)
  between operations  14.6 us (10%)
    all_to_all x1, blocking collectives, body(): lax.all_to_all(outgoing, 'ep', split_axis=0, concat_axis=0, tiled=True)  19.2 us
    ppermute x10, waiting for transfers between devices, reduce_stage(): lax.ppermute(sent.astype(jnp.bfloat16), 'ep', shift_pairs(factors, axis,...  15.1 us
    unnamed x46, local copies, waits for them, and re-layouts  14.9 us
    all_to_all x1, waiting for transfers between devices, body(): lax.all_to_all(finished, 'ep', split_axis=0, concat_axis=0, tiled=True)  14 us
    ppermute x10, starting transfers between devices, reduce_stage(): lax.ppermute(sent.astype(jnp.bfloat16), 'ep', shift_pairs(factors, axis,...  10.8 us
    all_to_all x1, starting transfers between devices, body(): lax.all_to_all(jnp.stack(jnp.split(normed, lax.axis_size('ep'), axis=1),...  8.34 us
    dot_general x1, matrix products, body(): jnp.einsum('xcf,xfd->xcd', hidden, w_expert_down, preferred_element_type=...  6.4 us
    reduce_sum x1, other arithmetic, memory_cell(): numerator = jnp.sum(new_matrix * query_heads[:, :, None, :], axis=-1)  6.34 us
  transfers between devices with their start and end apart: 17, of which 12 were waited for; matrix products, arithmetic and copies ran while one was open for 24% of the time, Pallas kernels for 0%

profile of v1, /device:TPU:0, one launch (start us, length us, event | category | flops | bytes accessed | tf_op | source)
XLA Modules:
  0.0 151.5 jit_solution(15241356886433280603)
XLA Ops:
  7.9 1.2 fusion.29
  19.8 8.3 %all-to-all-start = ((bf16[16,32,128]{2,1,0:T(8,128)(2,1)}), bf16[16,32,128]{2,1,0:T(8,128)(2,1)S(1)}, u32[]{:S(2)}, u32[]{:S(2)}) async-start(bf16[16,32,128]{2,1,0:T(8,128)(2,1)} %constant_dynamic-update-slice_fusion), calls=%async_computation | async-start | bytes 262144 | tf_op jit(solution)/shard_map/all_to_all | solution.py:152
  28.2 1.4 copy.58
  33.3 2.6 %all-to-all-done = bf16[16,32,128]{2,1,0:T(8,128)(2,1)S(1)} async-done(((bf16[16,32,128]{2,1,0:T(8,128)(2,1)}), bf16[16,32,128]{2,1,0:T(8,128)(2,1)S(1)}, u32[]{:S(2)}, u32[]{:S(2)}) %all-to-all-start) | async-done | bytes 131104 | tf_op jit(solution)/shard_map/all_to_all | solution.py:152
  35.9 1.2 convolution_convert_fusion.3
  37.9 1.1 collective-permute-start.5
  39.0 1.1 convolution_convert_fusion.2
  40.1 1.3 copy.57
  41.8 3.0 %collective-permute-done.5 = bf16[4,2,1,32,512]{4,3,2,1,0:T(8,128)(2,1)} collective-permute-done((bf16[4,2,1,32,512]{4,3,2,1,0:T(8,128)(2,1)}, bf16[4,2,1,32,512]{4,3,2,1,0:T(8,128)(2,1)}, u32[]{:S(2)}, u32[]{:S(2)}) %collective-permute-start.5) | collective-permute-done | bytes 262176 | tf_op jit(solution)/shard_map/ppermute | solution.py:88
  44.8 1.1 convert_add_fusion.1
  47.0 4.0 %collective-permute-done = bf16[4,1,2,32,520]{4,3,2,1,0:T(8,128)(2,1)S(1)} collective-permute-done((bf16[4,1,2,32,520]{4,3,2,1,0:T(8,128)(2,1)S(1)}, bf16[4,1,2,32,520]{4,3,2,1,0:T(8,128)(2,1)S(1)}, u32[]{:S(2)}, u32[]{:S(2)}) %collective-permute-start) | collective-permute-done | bytes 266272 | tf_op jit(solution)/shard_map/ppermute | solution.py:88
  52.8 3.6 %collective-permute-start.9 = (bf16[1,1,1,32,512]{4,3,2,1,0:T(8,128)(2,1)S(1)}, bf16[1,1,1,32,512]{4,3,2,1,0:T(8,128)(2,1)S(1)}, u32[]{:S(2)}, u32[]{:S(2)}) collective-permute-start(bf16[1,1,1,32,512]{4,3,2,1,0:T(8,128)(2,1)S(1)} %get-tuple-element.33), channel_id=1, source_target_pairs={{0,24},{2,26},{4,28},{6,30},{8,0},{10,2},{12,4},{14,6},{16,8},{18,... | collective-permute-start | bytes 98312 | tf_op jit(solution)/shard_map/ppermute | solution.py:88
  56.4 3.3 %collective-permute-done.1 = bf16[4,1,1,32,520]{4,3,2,1,0:T(8,128)(2,1)S(1)} collective-permute-done((bf16[4,1,1,32,520]{4,3,2,1,0:T(8,128)(2,1)S(1)}, bf16[4,1,1,32,520]{4,3,2,1,0:T(8,128)(2,1)S(1)}, u32[]{:S(2)}, u32[]{:S(2)}) %collective-permute-start.1) | collective-permute-done | bytes 133152 | tf_op jit(solution)/shard_map/ppermute | solution.py:88
  60.8 3.4 %collective-permute-start.4 = (bf16[1,1,1,32,520]{4,3,2,1,0:T(8,128)(2,1)}, bf16[1,1,1,32,520]{4,3,2,1,0:T(8,128)(2,1)S(1)}, u32[]{:S(2)}, u32[]{:S(2)}) collective-permute-start(bf16[1,1,1,32,520]{4,3,2,1,0:T(8,128)(2,1)} %get-tuple-element.30), channel_id=1, source_target_pairs={{0,24},{2,26},{4,28},{6,30},{8,0},{10,2},{12,4},{14,6},{16,8},{18,... | collective-permute-start | bytes 99848 | tf_op jit(solution)/shard_map/ppermute | solution.py:88
  64.4 1.9 %collective-permute-done.2 = bf16[1,1,1,32,520]{4,3,2,1,0:T(8,128)(2,1)S(1)} collective-permute-done((bf16[1,1,1,32,520]{4,3,2,1,0:T(8,128)(2,1)}, bf16[1,1,1,32,520]{4,3,2,1,0:T(8,128)(2,1)S(1)}, u32[]{:S(2)}, u32[]{:S(2)}) %collective-permute-start.2) | collective-permute-done | bytes 33312 | tf_op jit(solution)/shard_map/ppermute | solution.py:88
  67.0 2.2 %collective-permute-done.3 = bf16[1,1,1,32,520]{4,3,2,1,0:T(8,128)(2,1)} collective-permute-done((bf16[1,1,1,32,520]{4,3,2,1,0:T(8,128)(2,1)S(1)}, bf16[1,1,1,32,520]{4,3,2,1,0:T(8,128)(2,1)}, u32[]{:S(2)}, u32[]{:S(2)}) %collective-permute-start.3) | collective-permute-done | bytes 33312 | tf_op jit(solution)/shard_map/ppermute | solution.py:88
  71.8 1.6 %multiply_reduce_fusion.2 = (f32[32,4]{1,0:T(8,128)S(1)}, f32[32,4,64]{2,1,0:T(4,128)}, f32[32,4,64]{2,1,0:T(4,128)S(1)}, f32[32,4,64]{2,1,0:T(4,128)S(1)}) fusion(f32[32,4,64]{2,1,0:T(4,128)S(1)} %reshape.189, f32[32,4,64]{2,1,0:T(4,128)S(1)} %reshape.188, f32[32,4]{1,0:T(8,128)S(1)} %get-tuple-element.22, f32[32,4,64]{2,1,0:T(4,128)} %param.34, ...), kind=kLoop, calls=%fused_computation.65 | loop fusion | flops 57216 | bytes 231424 | tf_op jit(solution)/shard_map/reduce_sum | solution.py:43
  73.5 6.3 %multiply_reduce_fusion = (f32[32,4,64]{2,1,0:T(4,128)S(1)}, f32[32,4,64,64]{3,2,1,0:T(8,128)}) fusion(f32[32,4,64]{2,1,0:T(4,128)S(1)} %reshape.189, f32[32,4,64]{2,1,0:T(4,128)S(1)} %get-tuple-element.35, f32[32,4,64]{2,1,0:T(4,128)S(1)} %get-tuple-element.38, f32[32,4,64,64]{3,2,1,0:T(8,128)} %param.33, f32[32,4]{1,0:T(8,128)S(1)} %subtract_exponential_fusion.1), kind=kLoop, calls=%fused_computation | loop fusion | flops 2613248 | bytes 4325888 | tf_op jit(solution)/shard_map/reduce_sum | solution.py:42
  80.5 1.6 %convolution_convert_fusion.1 = bf16[32,2048]{1,0:T(8,128)(2,1)S(1)} fusion(bf16[256,2048]{1,0:T(8,128)(2,1)} %all-gather.2.cloned.1.call-done, f32[32,256]{1,0:T(8,128)S(1)} %mul.194, bf16[32,520]{1,0:T(8,128)(2,1)S(1)} %get-tuple-element.27, f32[256]{0:T(256)S(1)} %copy-done.10), kind=kOutput, calls=%fused_computation.13 | convolution fusion | flops 33677312 | bytes 1229824 | tf_op jit(solution)/shard_map/dot_general | solution.py:193
  82.3 1.2 collective-permute-done.10
  84.1 19.2 %all_to_all.15 = bf16[16,8,2048]{2,1,0:T(8,128)(2,1)S(1)} all-to-all(bf16[16,8,2048]{2,1,0:T(8,128)(2,1)S(1)} %fusion.12), channel_id=1, replica_groups=mesh['ep'=16,'tp'=2] {'ep'}, dimensions={0} | all-to-all | bytes 1048576 | tf_op jit(solution)/shard_map/all_to_all | solution.py:203
  103.2 1.9 %collective-permute-done.11 = bf16[16,8,2048]{2,1,0:T(8,128)(2,1)S(1)} collective-permute-done((bf16[16,8,2048]{2,1,0:T(8,128)(2,1)S(1)}, bf16[16,8,2048]{2,1,0:T(8,128)(2,1)S(1)}, u32[]{:S(2)}, u32[]{:S(2)}) %collective-permute-start.11) | collective-permute-done | bytes 524320 | tf_op jit(solution)/shard_map/ppermute | solution.py:103
  106.0 1.9 %fusion.4 = f32[256,704]{0,1:T(8,128)} fusion(bf16[1,2048,704]{1,2,0:T(8,128)(2,1)S(1)} %copy-done.11, bf16[1,128,2048]{2,1,0:T(8,128)(2,1)S(1)} %bitcast.121, bf16[1,128,2048]{2,1,0:T(8,128)(2,1)S(1)} %bitcast.119), kind=kOutput, calls=%fused_computation.6 | convolution fusion | flops 740294656 | bytes 4653056 | tf_op jit(solution)/shard_map/xcd,xdf->xcf/dot_general | solution.py:211
  107.8 6.4 %fusion.9 = bf16[1,256,2048]{2,1,0:T(8,128)(2,1)} fusion(bf16[1,704,2048]{2,1,0:T(8,128)(2,1)S(1)} %copy-done, bf16[1,2048,704]{1,2,0:T(8,128)(2,1)} %param.38, f32[256,704]{0,1:T(8,128)} %fusion.4, bf16[1,128,2048]{2,1,0:T(8,128)(2,1)} %bitcast.122, bf16[1,128,2048]{2,1,0:T(8,128)(2,1)S(1)} %bitcast.120), kind=kOutput, calls=%fused_computation.9 | convolution fusion | flops 1480097792 | bytes 8585216 | tf_op jit(solution)/shard_map/xcf,xfd->xcd/dot_general | solution.py:216
  115.5 1.8 %collective-permute-done.12 = bf16[1,128,2048]{2,1,0:T(8,128)(2,1)S(1)} collective-permute-done((bf16[1,128,2048]{2,1,0:T(8,128)(2,1)S(1)}, bf16[1,128,2048]{2,1,0:T(8,128)(2,1)S(1)}, u32[]{:S(2)}, u32[]{:S(2)}) %collective-permute-start.12) | collective-permute-done | bytes 524320 | tf_op jit(solution)/shard_map/ppermute | solution.py:103
  117.3 2.0 %fusion.24 = bf16[16,8,2048]{2,1,0:T(8,128)(2,1)} fusion(bf16[1,128,2048]{2,1,0:T(8,128)(2,1)S(1)} %collective-permute-done.12, bf16[1,256,2048]{2,1,0:T(8,128)(2,1)} %fusion.9), kind=kLoop, calls=%fused_computation.24 | loop fusion | flops 1048576 | bytes 1572864 | tf_op jit(solution)/shard_map/reshape;transpose;reshape | solution.py:226
  119.3 3.9 %all-to-all-start.2 = ((bf16[16,8,2048]{2,1,0:T(8,128)(2,1)}), bf16[16,8,2048]{2,1,0:T(8,128)(2,1)S(1)}, u32[]{:S(2)}, u32[]{:S(2)}) async-start(bf16[16,8,2048]{2,1,0:T(8,128)(2,1)} %fusion.24), calls=%async_computation.2 | async-start | bytes 1048576 | tf_op jit(solution)/shard_map/all_to_all | solution.py:227
  123.2 1.4 select_reduce_fusion
  124.6 14.0 %all-to-all-done.2 = bf16[16,8,2048]{2,1,0:T(8,128)(2,1)S(1)} async-done(((bf16[16,8,2048]{2,1,0:T(8,128)(2,1)}), bf16[16,8,2048]{2,1,0:T(8,128)(2,1)S(1)}, u32[]{:S(2)}, u32[]{:S(2)}) %all-to-all-start.2) | async-done | bytes 524320 | tf_op jit(solution)/shard_map/all_to_all | solution.py:227
  139.5 1.7 %convolution_add_fusion = f32[32,2048]{1,0:T(8,128)} fusion(f32[32,2048]{1,0:T(8,128)S(1)} %fusion.26, bf16[16,8,2048]{2,1,0:T(8,128)(2,1)S(1)} %all-to-all-done.2, f32[32,128]{1,0:T(8,128)} %select_reduce_fusion), kind=kOutput, calls=%fused_computation.12 | convolution fusion | flops 16859136 | bytes 1064960 | tf_op jit(solution)/shard_map/dot_general | solution.py:232
  141.9 1.1 collective-permute-done.13
  143.0 1.6 %fusion.36 = bf16[32,2048]{1,0:T(8,128)(2,1)} fusion(bf16[32,2048]{1,0:T(8,128)(2,1)S(1)} %get-tuple-element.17, f32[32,2048]{1,0:T(8,128)} %convolution_add_fusion, f32[32,2048]{1,0:T(8,128)S(1)} %collective-permute-done.13), kind=kLoop, calls=%fused_computation.45 | loop fusion | flops 262144 | bytes 786432 | tf_op jit(solution)/shard_map/convert_element_type | solution.py:236
  (105 shorter events, 28.5 us)
Async XLA Ops:
  7.2 100.7 %copy-start = (bf16[1,704,2048]{2,1,0:T(8,128)(2,1)S(1)}, bf16[1,704,2048]{2,1,0:T(8,128)(2,1)}, u32[]{:S(2)}) copy-start(bf16[1,704,2048]{2,1,0:T(8,128)(2,1)} %param.39) | copy-start | bytes 8650756
  7.2 31.8 %copy-start.3 = (bf16[128,256]{1,0:T(8,128)(2,1)S(1)}, bf16[128,256]{1,0:T(8,128)(2,1)}, u32[]{:S(2)}) copy-start(bf16[128,256]{1,0:T(8,128)(2,1)} %param.26) | copy-start | bytes 196612
  7.2 31.8 %copy-start.4 = (bf16[128,256]{1,0:T(8,128)(2,1)S(1)}, bf16[128,256]{1,0:T(8,128)(2,1)}, u32[]{:S(2)}) copy-start(bf16[128,256]{1,0:T(8,128)(2,1)} %param.25) | copy-start | bytes 196612
  7.2 73.3 %all-gather.2.cloned.1.call-start = ((), (), s32[]{:S(2)}) async-start(), calls=%async_computation.3 | async-start | bytes 1114112 | tf_op jit(solution)/shard_map/all_gather | solution.py:132
  19.8 16.1 %all-to-all-start = ((bf16[16,32,128]{2,1,0:T(8,128)(2,1)}), bf16[16,32,128]{2,1,0:T(8,128)(2,1)S(1)}, u32[]{:S(2)}, u32[]{:S(2)}) async-start(bf16[16,32,128]{2,1,0:T(8,128)(2,1)} %constant_dynamic-update-slice_fusion), calls=%async_computation | async-start | bytes 262144 | tf_op jit(solution)/shard_map/all_to_all | solution.py:152
  37.1 1.9 %copy-start.1 = (bf16[512,512]{1,0:T(8,128)(2,1)}, bf16[512,512]{1,0:T(8,128)(2,1)S(1)}, u32[]{:S(2)}) copy-start(bf16[512,512]{1,0:T(8,128)(2,1)S(1)} %convolution_convert_fusion.3) | copy-start | bytes 1572868
  37.9 6.9 %collective-permute-start.5 = (bf16[4,2,1,32,512]{4,3,2,1,0:T(8,128)(2,1)}, bf16[4,2,1,32,512]{4,3,2,1,0:T(8,128)(2,1)}, u32[]{:S(2)}, u32[]{:S(2)}) collective-permute-start(bf16[4,2,1,32,512]{4,3,2,1,0:T(8,128)(2,1)} %constant_dynamic-slice_fusion), channel_id=1, source_target_pairs={{0,2},{2,0},{4,6},{6,4},{8,10},{10,8},{12,14},{14,12},{16,18},{18,... | collective-permute-start | bytes 786440 | tf_op jit(solution)/shard_map/ppermute | solution.py:88
  41.5 9.5 %collective-permute-start = (bf16[4,1,2,32,520]{4,3,2,1,0:T(8,128)(2,1)S(1)}, bf16[4,1,2,32,520]{4,3,2,1,0:T(8,128)(2,1)S(1)}, u32[]{:S(2)}, u32[]{:S(2)}) collective-permute-start(bf16[4,1,2,32,520]{4,3,2,1,0:T(8,128)(2,1)S(1)} %constant_dynamic-slice_fusion.1), channel_id=1, source_target_pairs={{0,4},{2,6},{4,0},{6,2},{8,12},{10,14},{12,8},{14,10},{16,20},{18,... | collective-permute-start | bytes 798728 | tf_op jit(solution)/shard_map/ppermute | solution.py:88
  46.0 6.5 %collective-permute-start.6 = (bf16[4,1,1,32,512]{4,3,2,1,0:T(8,128)(2,1)S(1)}, bf16[4,1,1,32,512]{4,3,2,1,0:T(8,128)(2,1)S(1)}, u32[]{:S(2)}, u32[]{:S(2)}) collective-permute-start(bf16[4,1,1,32,512]{4,3,2,1,0:T(8,128)(2,1)S(1)} %dynamic-slice_convert_fusion.1), channel_id=1, source_target_pairs={{0,4},{2,6},{4,0},{6,2},{8,12},{10,14},{12,8},{14,10},{16,20},{18,... | collective-permute-start | bytes 393224 | tf_op jit(solution)/shard_map/ppermute | solution.py:88
  51.1 8.5 %collective-permute-start.1 = (bf16[4,1,1,32,520]{4,3,2,1,0:T(8,128)(2,1)S(1)}, bf16[4,1,1,32,520]{4,3,2,1,0:T(8,128)(2,1)S(1)}, u32[]{:S(2)}, u32[]{:S(2)}) collective-permute-start(bf16[4,1,1,32,520]{4,3,2,1,0:T(8,128)(2,1)S(1)} %dynamic-slice_convert_fusion), channel_id=1, source_target_pairs={{0,2},{2,0},{4,6},{6,4},{8,10},{10,8},{12,14},{14,12},{16,18},{18,... | collective-permute-start | bytes 399368 | tf_op jit(solution)/shard_map/ppermute | solution.py:88
  52.5 11.7 %collective-permute-start.7 = (bf16[1,1,1,32,512]{4,3,2,1,0:T(8,128)(2,1)S(1)}, bf16[1,1,1,32,512]{4,3,2,1,0:T(8,128)(2,1)S(1)}, u32[]{:S(2)}, u32[]{:S(2)}) collective-permute-start(bf16[1,1,1,32,512]{4,3,2,1,0:T(8,128)(2,1)S(1)} %get-tuple-element.32), channel_id=1, source_target_pairs={{0,8},{2,10},{4,12},{6,14},{8,16},{10,18},{12,20},{14,22},{16,24},... | collective-permute-start | bytes 98312 | tf_op jit(solution)/shard_map/ppermute | solution.py:88
  52.8 11.4 %collective-permute-start.9 = (bf16[1,1,1,32,512]{4,3,2,1,0:T(8,128)(2,1)S(1)}, bf16[1,1,1,32,512]{4,3,2,1,0:T(8,128)(2,1)S(1)}, u32[]{:S(2)}, u32[]{:S(2)}) collective-permute-start(bf16[1,1,1,32,512]{4,3,2,1,0:T(8,128)(2,1)S(1)} %get-tuple-element.33), channel_id=1, source_target_pairs={{0,24},{2,26},{4,28},{6,30},{8,0},{10,2},{12,4},{14,6},{16,8},{18,... | collective-permute-start | bytes 98312 | tf_op jit(solution)/shard_map/ppermute | solution.py:88
  56.4 7.8 %collective-permute-start.8 = (bf16[1,1,1,32,512]{4,3,2,1,0:T(8,128)(2,1)S(1)}, bf16[1,1,1,32,512]{4,3,2,1,0:T(8,128)(2,1)S(1)}, u32[]{:S(2)}, u32[]{:S(2)}) collective-permute-start(bf16[1,1,1,32,512]{4,3,2,1,0:T(8,128)(2,1)S(1)} %get-tuple-element.34), channel_id=1, source_target_pairs={{0,16},{2,18},{4,20},{6,22},{8,24},{10,26},{12,28},{14,30},{16,0},... | collective-permute-start | bytes 98312 | tf_op jit(solution)/shard_map/ppermute | solution.py:88
  60.3 6.0 %collective-permute-start.2 = (bf16[1,1,1,32,520]{4,3,2,1,0:T(8,128)(2,1)}, bf16[1,1,1,32,520]{4,3,2,1,0:T(8,128)(2,1)S(1)}, u32[]{:S(2)}, u32[]{:S(2)}) collective-permute-start(bf16[1,1,1,32,520]{4,3,2,1,0:T(8,128)(2,1)} %get-tuple-element.29), channel_id=1, source_target_pairs={{0,8},{2,10},{4,12},{6,14},{8,16},{10,18},{12,20},{14,22},{16,24},... | collective-permute-start | bytes 99848 | tf_op jit(solution)/shard_map/ppermute | solution.py:88
  60.8 5.6 %collective-permute-start.4 = (bf16[1,1,1,32,520]{4,3,2,1,0:T(8,128)(2,1)}, bf16[1,1,1,32,520]{4,3,2,1,0:T(8,128)(2,1)S(1)}, u32[]{:S(2)}, u32[]{:S(2)}) collective-permute-start(bf16[1,1,1,32,520]{4,3,2,1,0:T(8,128)(2,1)} %get-tuple-element.30), channel_id=1, source_target_pairs={{0,24},{2,26},{4,28},{6,30},{8,0},{10,2},{12,4},{14,6},{16,8},{18,... | collective-permute-start | bytes 99848 | tf_op jit(solution)/shard_map/ppermute | solution.py:88
  64.2 5.0 %collective-permute-start.3 = (bf16[1,1,1,32,520]{4,3,2,1,0:T(8,128)(2,1)S(1)}, bf16[1,1,1,32,520]{4,3,2,1,0:T(8,128)(2,1)}, u32[]{:S(2)}, u32[]{:S(2)}) collective-permute-start(bf16[1,1,1,32,520]{4,3,2,1,0:T(8,128)(2,1)S(1)} %get-tuple-element.31), channel_id=1, source_target_pairs={{0,16},{2,18},{4,20},{6,22},{8,24},{10,26},{12,28},{14,30},{16,0},... | collective-permute-start | bytes 99848 | tf_op jit(solution)/shard_map/ppermute | solution.py:88
  66.4 0.6 copy-start.5
  73.4 7.1 %copy-start.10 = (f32[256]{0:T(256)S(1)}, f32[256]{0:T(256)}, u32[]{:S(2)}) copy-start(f32[256]{0:T(256)} %param.31) | copy-start | bytes 3076
  73.4 8.8 %copy-start.8 = (s32[32,3]{0,1:T(4,128)S(1)}, s32[32,3]{0,1:T(4,128)}, u32[]{:S(2)}) copy-start(s32[32,3]{0,1:T(4,128)} %param.40) | copy-start | bytes 1156
  73.4 8.7 %copy-start.9 = (s32[32,3]{0,1:T(4,128)S(1)}, s32[32,3]{0,1:T(4,128)}, u32[]{:S(2)}) copy-start(s32[32,3]{0,1:T(4,128)} %copy.60) | copy-start | bytes 1156
  73.4 10.1 %copy-start.2 = (bf16[32,2048]{1,0:T(8,128)(2,1)S(1)}, bf16[32,2048]{1,0:T(8,128)(2,1)}, u32[]{:S(2)}) copy-start(bf16[32,2048]{1,0:T(8,128)(2,1)} %param.21) | copy-start | bytes 393220
  73.5 10.2 %copy-start.7 = (f32[2048]{0:T(1024)S(1)}, f32[2048]{0:T(1024)}, u32[]{:S(2)}) copy-start(f32[2048]{0:T(1024)} %param.36) | copy-start | bytes 24580
  80.5 25.5 %copy-start.11 = (bf16[1,2048,704]{1,2,0:T(8,128)(2,1)S(1)}, bf16[1,2048,704]{1,2,0:T(8,128)(2,1)}, u32[]{:S(2)}) copy-start(bf16[1,2048,704]{1,2,0:T(8,128)(2,1)} %param.37) | copy-start | bytes 8650756
  82.1 1.4 collective-permute-start.10
  82.2 1.5 copy-start.6
  103.2 1.9 %collective-permute-start.11 = (bf16[16,8,2048]{2,1,0:T(8,128)(2,1)S(1)}, bf16[16,8,2048]{2,1,0:T(8,128)(2,1)S(1)}, u32[]{:S(2)}, u32[]{:S(2)}) collective-permute-start(bf16[16,8,2048]{2,1,0:T(8,128)(2,1)S(1)} %all_to_all.15), channel_id=1, source_target_pairs={{0,1},{1,0},{2,3},{3,2},{4,5},{5,4},{6,7},{7,6},{8,9},{9,8},{10,11... | collective-permute-start | bytes 1572872 | tf_op jit(solution)/shard_map/ppermute | solution.py:103
  105.2 0.8 copy-start.12
  115.3 2.0 %collective-permute-start.12 = (bf16[1,128,2048]{2,1,0:T(8,128)(2,1)S(1)}, bf16[1,128,2048]{2,1,0:T(8,128)(2,1)S(1)}, u32[]{:S(2)}, u32[]{:S(2)}) collective-permute-start(bf16[1,128,2048]{2,1,0:T(8,128)(2,1)S(1)} %slice.43), channel_id=1, source_target_pairs={{0,1},{1,0},{2,3},{3,2},{4,5},{5,4},{6,7},{7,6},{8,9},{9,8},{10,11... | collective-permute-start | bytes 1572872 | tf_op jit(solution)/shard_map/ppermute | solution.py:103
  119.3 19.3 %all-to-all-start.2 = ((bf16[16,8,2048]{2,1,0:T(8,128)(2,1)}), bf16[16,8,2048]{2,1,0:T(8,128)(2,1)S(1)}, u32[]{:S(2)}, u32[]{:S(2)}) async-start(bf16[16,8,2048]{2,1,0:T(8,128)(2,1)} %fusion.24), calls=%async_computation.2 | async-start | bytes 1048576 | tf_op jit(solution)/shard_map/all_to_all | solution.py:227
  141.2 1.7 %collective-permute-start.13 = (f32[32,2048]{1,0:T(8,128)}, f32[32,2048]{1,0:T(8,128)S(1)}, u32[]{:S(2)}, u32[]{:S(2)}) collective-permute-start(f32[32,2048]{1,0:T(8,128)} %convolution_add_fusion), channel_id=1, source_target_pairs={{0,1},{1,0},{2,3},{3,2},{4,5},{5,4},{6,7},{7,6},{8,9},{9,8},{10,11... | collective-permute-start | bytes 786440 | tf_op jit(solution)/shard_map/ppermute | solution.py:103
Sparse Core Ops, SparseCore 0:
  10.7 57.7 all-gather.1
